TPU v7x, 32 devices: a whole 2x2x4 slice. The times are simulated.
32 devices in a mesh: grp: 2 (over y), sp: 4 (over z), tp: 4 (over x, core).
Axes of the slice: x: 2, y: 2, z: 4, core: 2. Of those that a mesh axis runs over, the one named last changes fastest.
Arguments:
- ssm_input: bfloat16 [1024, 1024], P(('grp', 'sp'), 'tp'), parts along dimension 0, may hold values from -6 to 6
- residual_in: bfloat16 [1024, 2048], P(('grp', 'sp')), parts along dimension 0, may hold values from -4 to 4
- log_step: float32 [64], P('tp'), may hold values from -6.91 to -2.3
- decay_real: float32 [64, 64], P('tp'), may hold values from -34 to 0, as said below
- freq: float32 [64, 64], P('tp'), may hold values from 0.5 to 8
- in_real: float32 [64, 64, 16], P('tp'), may hold values from -1 to 1
- in_imag: float32 [64, 64, 16], P('tp'), may hold values from -1 to 1
- out_real: float32 [64, 16, 64], P('tp'), may hold values from -0.5 to 0.5
- out_imag: float32 [64, 16, 64], P('tp'), may hold values from -0.5 to 0.5
- skip: float32 [1024], P('tp'), may hold values from -3 to 3
- w_glu: bfloat16 [1024, 1024], replicated, may hold values from -0.1875 to 0.1875
- b_glu: float32 [1024], replicated, may hold values from -3 to 3
- w_branch: bfloat16 [1024, 2048], replicated, may hold values from -0.1875 to 0.1875
- norm_gain: float32 [2048], replicated, may hold values from 0.1 to 1.9
- w_gate: bfloat16 [2048, 5632], P('sp', 'tp'), may hold values from -0.125 to 0.125
- w_up: bfloat16 [2048, 5632], P('sp', 'tp'), may hold values from -0.125 to 0.125
- w_down: bfloat16 [5632, 2048], P('tp', 'sp'), may hold values from -0.078125 to 0.078125
Outputs:
- mixed: bfloat16 [1024, 2048], P(('grp', 'sp', 'tp')), parts along dimension 0
There are 2 independent parts, one for each index of `grp`. A program takes and returns all parts, laid end to end along the dimension named above; an argument that names none is the same for every part. Nothing has to cross between parts.
Inputs may be any that keep to these rules, and one draw needn't show every extreme that they name: `decay_real`: negative in every entry.
All inputs are finite; a program needn't handle non-finite values.
Results may differ from a plain program's by a relative error of at most 0.015.
Values may be sent and summed in bfloat16 or wider, within the bound.
No kernel may reach another device: no remote copies, remote signals or barrier semaphores. Data moves between devices by JAX's collectives and lax.ppermute only.
A program may use at most 128 MiB of HBM per device.

v0:
```python
import math

import jax
import jax.numpy as jnp
from jax import lax
from jax.experimental import pallas as pl
from jax.experimental.pallas import tpu as pltpu
from jax.sharding import PartitionSpec as P

EPS = 1e-06


def prefix(shard, axis, combine, identity):
    count, place = (lax.axis_size(axis), lax.axis_index(axis))
    everything = tuple(jnp.moveaxis(lax.all_gather(jnp.stack(shard), axis), 1, 0))
    start = jax.tree.map(
        lambda part, zero: jnp.broadcast_to(jnp.asarray(zero, part.dtype), part.shape),
        shard,
        identity,
    )

    def lap(k, before):
        reached = k < place
        new = combine(before, tuple(part[k] for part in everything))
        return jax.tree.map(lambda a, b: jnp.where(reached, a, b), new, before)

    return lax.fori_loop(0, count, lap, start)


def discretize(log_step, decay_real, freq, in_real, in_imag):
    step_size = jnp.exp(log_step)[:, None]
    magnitude = jnp.exp(decay_real * step_size)
    abar_re = magnitude * jnp.cos(freq * step_size)
    abar_im = magnitude * jnp.sin(freq * step_size)
    denominator = decay_real * decay_real + freq * freq
    less_re = abar_re - 1.0
    hold_re = ((less_re * decay_real + abar_im * freq) / denominator)[..., None]
    hold_im = ((abar_im * decay_real - less_re * freq) / denominator)[..., None]
    bbar_re = hold_re * in_real - hold_im * in_imag
    bbar_im = hold_re * in_imag + hold_im * in_real
    return (step_size, abar_re, abar_im, bbar_re, bbar_im)


def powers(decay_real, freq, step_size, length):
    steps_up = (jnp.arange(length, dtype=jnp.int32) + 1).astype(jnp.float32)[:, None, None]
    magnitude = jnp.exp((decay_real * step_size)[None] * steps_up)
    phase = (freq * step_size)[None] * steps_up
    return (magnitude * jnp.cos(phase), magnitude * jnp.sin(phase))


def compose(earlier, later):
    a1r, a1i, b1r, b1i = earlier
    a2r, a2i, b2r, b2i = later
    return (
        a2r * a1r - a2i * a1i,
        a2r * a1i + a2i * a1r,
        a2r * b1r - a2i * b1i + b2r,
        a2r * b1i + a2i * b1r + b2i,
    )


def local_states(inputs, decay_real, freq, step_size, bbar_re, bbar_im):
    highest = lax.Precision.HIGHEST
    tok_rows, group_count, _ = inputs.shape
    lanes = group_count * decay_real.shape[1]
    drive_re = jnp.einsum("lgm,gpm->lgp", inputs, bbar_re, precision=highest).reshape(
        tok_rows, lanes
    )
    drive_im = jnp.einsum("lgm,gpm->lgp", inputs, bbar_im, precision=highest).reshape(
        tok_rows, lanes
    )
    span = math.gcd(tok_rows, 16)
    spans = tok_rows // span
    rate = (decay_real * step_size).reshape(lanes)
    turn = (freq * step_size).reshape(lanes)
    later = jnp.arange(span, dtype=jnp.int32)[:, None]
    earlier = jnp.arange(span, dtype=jnp.int32)[None, :]
    lag = (later - earlier).astype(jnp.float32)
    causal = (later >= earlier)[..., None]
    lag_pos = jnp.maximum(lag, 0.0)[..., None]
    table_mag = jnp.exp(rate[None, None] * lag_pos)
    table_re = jnp.where(causal, table_mag * jnp.cos(turn[None, None] * lag_pos), 0.0)
    table_im = jnp.where(causal, table_mag * jnp.sin(turn[None, None] * lag_pos), 0.0)
    block_re = drive_re.reshape(spans, 1, span, lanes)
    block_im = drive_im.reshape(spans, 1, span, lanes)
    inner_re = jnp.sum(table_re[None] * block_re - table_im[None] * block_im, axis=2)
    inner_im = jnp.sum(table_re[None] * block_im + table_im[None] * block_re, axis=2)
    steps_up = (jnp.arange(span, dtype=jnp.int32) + 1).astype(jnp.float32)[:, None]
    pow_mag = jnp.exp(rate[None] * steps_up)
    pow_re = pow_mag * jnp.cos(turn[None] * steps_up)
    pow_im = pow_mag * jnp.sin(turn[None] * steps_up)
    span_re = pow_re[-1]
    span_im = pow_im[-1]

    def carry_step(entering, ends):
        next_re = span_re * entering[0] - span_im * entering[1] + ends[0]
        next_im = span_re * entering[1] + span_im * entering[0] + ends[1]
        return ((next_re, next_im), entering)

    zeros = jnp.zeros((lanes,), jnp.float32)
    _, entering = lax.scan(
        carry_step, (zeros, zeros), (inner_re[:, -1], inner_im[:, -1])
    )
    state_re = inner_re + pow_re[None] * entering[0][:, None] - pow_im[None] * entering[1][:, None]
    state_im = inner_im + pow_re[None] * entering[1][:, None] + pow_im[None] * entering[0][:, None]
    shape = (tok_rows, group_count, decay_real.shape[1])
    return (state_re.reshape(shape), state_im.reshape(shape))


def readout(state_re, state_im, out_real, out_imag, skip_mat, inputs):
    highest = lax.Precision.HIGHEST
    values = (
        jnp.einsum("lgp,gmp->lgm", state_re, out_real, precision=highest)
        - jnp.einsum("lgp,gmp->lgm", state_im, out_imag, precision=highest)
        + skip_mat[None] * inputs
    )
    values = jax.nn.gelu(values)
    return values.reshape(values.shape[0], -1).astype(jnp.bfloat16)


def row_norm(stream, norm_gain):
    scale_rows = lax.rsqrt(jnp.mean(stream * stream, axis=-1, keepdims=True) + EPS)
    return (stream * scale_rows * norm_gain).astype(jnp.bfloat16)


LANES = 128


def can_reshard(tok_rows, group_count, in_shape, w_gate, w_down):
    planes, parts, cores = (lax.axis_size("sp"), lax.axis_size("grp"), lax.axis_size("tp"))
    rows, units = w_gate.shape
    width = tile_width(units, planes)
    return (
        2 < planes <= 8
        and parts == 2
        and cores == 4
        and units >= width
        and rows % (2 * LANES) == 0
        and w_down.shape[1] % (2 * LANES) == 0
        and tok_rows % (cores * 16) == 0
        and tok_rows & (tok_rows - 1) == 0
        and group_count * in_shape[1] % LANES == 0
        and group_count * in_shape[2] % LANES == 0
    )


def tile_width(units, planes):
    return -(-(-(-units // planes)) // LANES) * LANES


def hop(value, axis, distance):
    count = lax.axis_size(axis)
    return lax.ppermute(value, axis, [(i, (i + distance) % count) for i in range(count)])


def swap(value, axis, bit):
    return lax.ppermute(value, axis, [(i, i ^ bit) for i in range(lax.axis_size(axis))])


def halves(value):
    high = value.astype(jnp.bfloat16)
    return (high, (value - high.astype(jnp.float32)).astype(jnp.bfloat16))


def across(a, b):
    return lax.dot_general(a, b, (((1,), (1,)), ((), ())), preferred_element_type=jnp.float32)


def times(a, b):
    return (a[0] * b[0] - a[1] * b[1], a[0] * b[1] + a[1] * b[0])


def repeated(value, copies):
    size = value.shape[1]
    shape = (size, copies * size)
    pick = lax.broadcasted_iota(jnp.int32, shape, 0) == lax.broadcasted_iota(jnp.int32, shape, 1) % size
    return jnp.dot(value, pick.astype(jnp.bfloat16), preferred_element_type=jnp.float32)


def block_diagonal(value, groups):
    rows, size = (value.shape[0] // groups, value.shape[1])
    shape = (value.shape[0], groups * size)
    own = lax.broadcasted_iota(jnp.int32, shape, 0) // rows == lax.broadcasted_iota(jnp.int32, shape, 1) // size
    return [jnp.where(own, repeated(part, groups), 0.0).astype(jnp.bfloat16) for part in halves(value)]


def local_scan(ssm_input, log_step, decay_real, freq, in_real, in_imag):
    length = ssm_input.shape[0]
    groups, states, size = in_real.shape
    lanes = groups * states

    def kernel(log_ref, x, decay_ref, freq_ref, in_re, in_im, out_re, out_im, end, abar, hold):
        row = lax.broadcasted_iota(jnp.int32, (groups, states), 0)
        log = jnp.zeros((groups, states), jnp.float32)
        for g in range(groups):
            log = jnp.where(row == g, log_ref[g], log)
        step = jnp.exp(log)
        decay, turn = (decay_ref[...], freq_ref[...])
        magnitude = jnp.exp(decay * step)
        abar_re = magnitude * jnp.cos(turn * step)
        abar_im = magnitude * jnp.sin(turn * step)
        denominator = decay * decay + turn * turn
        less_re = abar_re - 1.0
        hold_re = (less_re * decay + abar_im * turn) / denominator
        hold_im = (abar_im * decay - less_re * turn) / denominator
        shape = (states, lanes)
        pick = lax.broadcasted_iota(jnp.int32, shape, 0) == lax.broadcasted_iota(jnp.int32, shape, 1) % states
        own = lax.broadcasted_iota(jnp.int32, (groups, lanes), 0) == (
            lax.broadcasted_iota(jnp.int32, (groups, lanes), 1) // states
        )
        for target, k, value in ((abar, 0, abar_re), (abar, 1, abar_im), (hold, 0, hold_re), (hold, 1, hold_im)):
            wide = jnp.dot(
                value, pick.astype(jnp.float32), preferred_element_type=jnp.float32, precision=lax.Precision.HIGHEST
            )
            target[k : k + 1, :] = jnp.sum(jnp.where(own, wide, 0.0), axis=0, keepdims=True)
        rows = x[...]
        for target, source in ((out_re, in_re), (out_im, in_im)):
            high, low = block_diagonal(source[...], groups)
            target[...] = jnp.dot(rows, high, preferred_element_type=jnp.float32) + jnp.dot(
                rows, low, preferred_element_type=jnp.float32
            )
        place = lax.broadcasted_iota(jnp.int32, (length, LANES), 0)
        for first in range(0, lanes, LANES):
            at = slice(first, first + LANES)
            power = (abar[0:1, at], abar[1:2, at])
            state = times((hold[0:1, at], hold[1:2, at]), (out_re[:, at], out_im[:, at]))
            gap = 1
            while gap < length:
                late = place >= gap
                before = tuple(jnp.where(late, pltpu.roll(part, gap, 0), 0.0) for part in state)
                moved = times(power, before)
                state = (state[0] + moved[0], state[1] + moved[1])
                power = times(power, power)
                gap *= 2
            out_re[:, at], out_im[:, at] = state
            end[0:1, at] = state[0][length - 1 :]
            end[1:2, at] = state[1][length - 1 :]

    pair = jax.ShapeDtypeStruct((2, lanes), jnp.float32)
    whole = jax.ShapeDtypeStruct((length, lanes), jnp.float32)
    vmem = pl.BlockSpec()
    return pl.pallas_call(
        kernel,
        grid=(1,),
        in_specs=[pl.BlockSpec(memory_space=pltpu.SMEM)] + [vmem] * 5,
        out_specs=[vmem] * 4,
        out_shape=[whole, whole, pair, pair],
        scratch_shapes=[pltpu.VMEM((2, lanes), jnp.float32)],
        compiler_params=pltpu.CompilerParams(vmem_limit_bytes=20 * 1024 * 1024),
        name="local_scan",
    )(
        log_step,
        ssm_input,
        decay_real,
        freq,
        jnp.swapaxes(in_real, 1, 2).reshape(groups * size, states),
        jnp.swapaxes(in_imag, 1, 2).reshape(groups * size, states),
    )


def mixed_out(state_re, state_im, abar, ends, out_real, out_imag, skip, ssm_input):
    length, lanes = state_re.shape
    groups, size, states = out_real.shape
    span = 8

    def kernel(*refs):
        s_re, s_im, abar_ref = refs[:3]
        end_refs = refs[3 : 3 + len(ends)]
        o_re, o_im, skip_ref, x, out = refs[3 + len(ends) : 8 + len(ends)]
        full_re, full_im = refs[8 + len(ends) :]
        for first in range(0, lanes, LANES):
            at = slice(first, first + LANES)
            one = (abar_ref[0:1, at], abar_ref[1:2, at])
            count = lax.broadcasted_iota(jnp.int32, (span, LANES), 0) + 1
            table = (jnp.ones((span, LANES), jnp.float32), jnp.zeros((span, LANES), jnp.float32))
            power, gap = (one, 1)
            while gap < length:
                if gap == span:
                    eight = power
                if gap <= span:
                    more = times(table, power)
                    odd = (count // gap) % 2 == 1
                    table = tuple(jnp.where(odd, a, b) for a, b in zip(more, table))
                power = times(power, power)
                gap *= 2
            carry = None
            for end in reversed(end_refs):
                here = (end[0:1, at], end[1:2, at])
                if carry is None:
                    carry = here
                else:
                    moved = times(power, carry)
                    carry = (here[0] + moved[0], here[1] + moved[1])
            table = times(table, carry)
            for start in range(0, length, span):
                rows = slice(start, start + span)
                full_re[rows, at] = s_re[rows, at] + table[0]
                full_im[rows, at] = s_im[rows, at] + table[1]
                table = times(table, eight)
        re_high, re_low = halves(full_re[...])
        im_high, im_low = halves(full_im[...])
        cre_high, cre_low = block_diagonal(o_re[...], groups)
        cim_high, cim_low = block_diagonal(o_im[...], groups)
        value = across(re_high, cre_high) + across(re_low, cre_high) + across(re_high, cre_low)
        value -= across(im_high, cim_high) + across(im_low, cim_high) + across(im_high, cim_low)
        value += skip_ref[...] * x[...].astype(jnp.float32)
        out[...] = jax.nn.gelu(value).astype(jnp.bfloat16)

    vmem = pl.BlockSpec()
    return pl.pallas_call(
        kernel,
        grid=(1,),
        in_specs=[vmem] * (7 + len(ends)),
        out_specs=vmem,
        out_shape=jax.ShapeDtypeStruct((length, groups * size), jnp.bfloat16),
        scratch_shapes=[pltpu.VMEM((length, lanes), jnp.float32)] * 2,
        compiler_params=pltpu.CompilerParams(vmem_limit_bytes=20 * 1024 * 1024),
        name="mixed_out",
    )(
        state_re,
        state_im,
        abar,
        *ends,
        out_real.reshape(groups * size, states),
        out_imag.reshape(groups * size, states),
        skip.reshape(1, -1),
        ssm_input,
    )


def mixer(ssm_input, log_step, decay_real, freq, in_real, in_imag, out_real, out_imag, skip):
    planes = lax.axis_size("sp")
    state_re, state_im, end, abar = local_scan(ssm_input, log_step, decay_real, freq, in_real, in_imag)
    ends = []
    for d in range(1, planes):
        ends.append(lax.ppermute(end, "sp", [(i, i + d) for i in range(planes - d)]))
    return mixed_out(state_re, state_im, abar, ends, out_real, out_imag, skip, ssm_input)


def first_unit(plane, planes, units):
    width = tile_width(units, planes)
    return jnp.minimum(plane * width, units - width)


def run_copies(copies, sems):
    copies = [pltpu.make_async_copy(a, b, sems.at[i]) for i, (a, b) in enumerate(copies)]
    for copy in copies:
        copy.start()
    for copy in copies:
        copy.wait()


def cut(w_gate, w_up, w_down, wide_at, tall_at, grant):
    planes = lax.axis_size("sp")
    rows, units = w_gate.shape
    cols = w_down.shape[1]
    width = tile_width(units, planes)
    count = len(wide_at)

    def kernel(gate, up, down, *refs):
        wides, talls = (refs[:count], refs[count:-1])
        place, part = (lax.axis_index("sp"), lax.axis_index("grp"))
        row = pl.ds(pl.multiple_of(part * (rows // 2), LANES), rows // 2)
        col = pl.ds(pl.multiple_of(part * (cols // 2), LANES), cols // 2)

        def units_of(d):
            first = first_unit((place + d) % planes, planes, units)
            return pl.ds(pl.multiple_of(first, LANES), width)

        copies = []
        for (d, what), wide in zip(wide_at, wides):
            r = row if d else slice(None)
            sources = [w for w, name in ((gate, "gate"), (up, "up")) if what in (name, "both")]
            for i, source in enumerate(sources):
                copies.append((source.at[r, units_of(d)], wide.at[:, pl.ds(i * width, width)]))
        for d, tall in zip(tall_at, talls):
            copies.append((down.at[units_of(d), col if d else slice(None)], tall))
        run_copies(copies, refs[-1])

    anywhere = pl.BlockSpec(memory_space=pltpu.HBM)
    shapes = [
        (rows // 2 if d else rows, 2 * width if what == "both" else width) for d, what in wide_at
    ]
    shapes += [(width, cols // 2 if d else cols) for d in tall_at]
    pieces = pl.pallas_call(
        kernel,
        in_specs=[anywhere] * 3,
        out_specs=[pl.BlockSpec(memory_space=pltpu.VMEM)] * len(shapes),
        out_shape=[jax.ShapeDtypeStruct(shape, w_gate.dtype) for shape in shapes],
        scratch_shapes=[pltpu.SemaphoreType.DMA((2 * count + len(tall_at),))],
        compiler_params=pltpu.CompilerParams(vmem_limit_bytes=grant * 1024 * 1024),
    )(w_gate, w_up, w_down)
    return (dict(zip(wide_at, pieces[:count])), dict(zip(tall_at, pieces[count:])))


def reshard(w_gate, w_up, w_down):
    planes = lax.axis_size("sp")
    order = list(range(1, planes))
    last = order[-1]
    first, unused = cut(w_gate, w_up, w_down, [(1, "both"), (last, "gate")], [], 60)
    middle = [(d, "both") for d in order[1:-1]] + [(last, "up")]
    second, unused = cut(w_gate, w_up, w_down, middle, [], 60)
    third, talls = cut(w_gate, w_up, w_down, [(0, "both")], order + [0], 60)

    def spread(piece, d):
        if d == 0:
            return [(piece, swap(piece, "tp", 1))]
        mine = hop(piece, "sp", d)
        other = swap(mine, "grp", 1)
        return [(half, swap(half, "tp", 1)) for half in (mine, other)]

    wides = []
    for (d, what), piece in {**first, **second, **third}.items():
        wides += [(d, what, half, pair) for half, pair in enumerate(spread(piece, d))]
    return (wides, {d: spread(piece, d) for d, piece in talls.items()})


def gate_up(tokens, wides, core, units):
    planes = lax.axis_size("sp")
    whole = not isinstance(tokens, list)
    toks = [tokens] if whole else tokens
    rows, features = toks[0].shape
    count = rows * len(toks)
    block = features // planes
    width = tile_width(units, planes)
    pieces = [pair[core] for unused_d, unused_what, unused_half, pair in wides]

    def kernel(*refs):
        place, part = (lax.axis_index("sp"), lax.axis_index("grp"))
        spots = []
        for d, what, half, unused in wides:
            start = (place - d + planes) % planes * block
            if d:
                start += (1 - part if half else part) * (block // 2)
            spots.append((start, width if what == "up" else 0))
        tok_refs, weights = (refs[: len(toks)], refs[len(toks) : len(toks) + len(pieces)])
        out, *outs, wide, sems = refs[len(toks) + len(pieces) :]
        tok = tok_refs[0] if whole else outs[0]
        copies = [] if whole else [(ref, tok.at[pl.ds(i * rows, rows), :]) for i, ref in enumerate(tok_refs)]
        for (start, col), weight in zip(spots, weights):
            row = pl.ds(pl.multiple_of(start, 16), weight.shape[0])
            copies.append((weight, wide.at[row, pl.ds(col, weight.shape[1])]))
        run_copies(copies, sems)
        sums = jnp.dot(tok[...], wide[...], preferred_element_type=jnp.float32)
        gate, up = (sums[:, :width], sums[:, width:])
        hidden = gate / (1.0 + jnp.exp(-gate)) * up
        live = lax.broadcasted_iota(jnp.int32, hidden.shape, 1) >= place * width - first_unit(
            place, planes, units
        )
        out[...] = jnp.where(live, hidden, 0.0).astype(jnp.bfloat16)

    anywhere = pl.BlockSpec(memory_space=pl.ANY)
    vmem = pl.BlockSpec(memory_space=pltpu.VMEM)
    shapes = [jax.ShapeDtypeStruct((count, width), jnp.bfloat16)]
    if not whole:
        shapes.append(jax.ShapeDtypeStruct((count, features), jnp.bfloat16))
    return pl.pallas_call(
        kernel,
        in_specs=[vmem if whole else anywhere] * len(toks) + [anywhere] * len(pieces),
        out_specs=[vmem] * len(shapes),
        out_shape=shapes,
        scratch_shapes=[
            pltpu.VMEM((features, 2 * width), jnp.bfloat16),
            pltpu.SemaphoreType.DMA((len(toks) + len(pieces),)),
        ],
        compiler_params=pltpu.CompilerParams(vmem_limit_bytes=16 * 1024 * 1024),
    )(*toks, *pieces)


def down(hiddens, talls, distances):
    count, width = hiddens[0].shape
    pairs = [pair for d in distances for pair in talls[d]]
    flat = [piece for pair in pairs for piece in pair]
    cols = sum(own.shape[1] for own, unused in pairs)
    kept = count // 2

    def kernel(own_hidden, other_hidden, *refs):
        weights = refs[: len(flat)]
        out_kept, out_sent, tall, sems = refs[len(flat) :]
        copies, at = ([], 0)
        for i, (own, unused) in enumerate(pairs):
            col = pl.ds(at, own.shape[1])
            copies += [(weights[2 * i + core], tall.at[core, :, col]) for core in range(2)]
            at += own.shape[1]
        run_copies(copies, sems)

        def product(rows):
            return jnp.dot(
                own_hidden[rows, :], tall[0], preferred_element_type=jnp.float32
            ) + jnp.dot(other_hidden[rows, :], tall[1], preferred_element_type=jnp.float32)

        out_sent[...] = product(slice(kept, count)).astype(jnp.bfloat16)
        out_kept[...] = product(slice(0, kept))

    anywhere = pl.BlockSpec(memory_space=pl.ANY)
    vmem = pl.BlockSpec(memory_space=pltpu.VMEM)
    return pl.pallas_call(
        kernel,
        in_specs=[vmem] * 2 + [anywhere] * len(flat),
        out_specs=[vmem, vmem],
        out_shape=[
            jax.ShapeDtypeStruct((kept, cols), jnp.float32),
            jax.ShapeDtypeStruct((count - kept, cols), jnp.bfloat16),
        ],
        scratch_shapes=[
            pltpu.VMEM((2, width, cols), jnp.bfloat16),
            pltpu.SemaphoreType.DMA((len(flat),)),
        ],
        compiler_params=pltpu.CompilerParams(vmem_limit_bytes=16 * 1024 * 1024),
    )(*hiddens, *flat)


def add_sums(kept, sent, count):
    rows, cols = (kept.shape[0] // count, kept.shape[1])

    def kernel(a, b, *outs):
        for i, out in enumerate(outs):
            at = slice(i * rows, (i + 1) * rows)
            out[...] = (a[at, :] + b[at, :].astype(jnp.float32)).astype(out.dtype)

    vmem = pl.BlockSpec(memory_space=pltpu.VMEM)
    return pl.pallas_call(
        kernel,
        in_specs=[vmem, vmem],
        out_specs=[vmem] * count,
        out_shape=[jax.ShapeDtypeStruct((rows, cols), jnp.float32)]
        + [jax.ShapeDtypeStruct((rows, cols), jnp.bfloat16)] * (count - 1),
        compiler_params=pltpu.CompilerParams(vmem_limit_bytes=8 * 1024 * 1024),
    )(kept, sent)


def gated_branch(blocks, w_glu, b_glu, w_branch, residual_in, norm_gain):
    senders, rows, channels = blocks.shape
    width, features = w_branch.shape

    def kernel(block, bias, gain, glu_hbm, branch_hbm, residual, out_stream, out_normed, mixed, own, glu, branch, sems):
        at = pl.ds(pl.multiple_of(lax.axis_index("tp") * rows, 16), rows)
        copies = [(glu_hbm, glu), (branch_hbm, branch), (residual.at[at, :], own)]
        copies = [pltpu.make_async_copy(a, b, sems.at[i]) for i, (a, b) in enumerate(copies)]
        for copy in copies:
            copy.start()
        for i in range(senders):
            mixed[:, i * channels : (i + 1) * channels] = block[i]
        copies[0].wait()
        pre = jnp.dot(mixed[...], glu[...], preferred_element_type=jnp.float32) + bias[...]
        gated = (mixed[...].astype(jnp.float32) * jax.nn.sigmoid(pre)).astype(jnp.bfloat16)
        for copy in copies[1:]:
            copy.wait()
        stream = own[...].astype(jnp.float32) + jnp.dot(
            gated, branch[...], preferred_element_type=jnp.float32
        )
        out_stream[...] = stream
        out_normed[...] = row_norm(stream, gain[...])

    vmem = pl.BlockSpec(memory_space=pltpu.VMEM)
    return pl.pallas_call(
        kernel,
        in_specs=[vmem] * 3 + [pl.BlockSpec(memory_space=pl.ANY)] * 3,
        out_specs=[vmem, vmem],
        out_shape=[
            jax.ShapeDtypeStruct((rows, features), jnp.float32),
            jax.ShapeDtypeStruct((rows, features), jnp.bfloat16),
        ],
        scratch_shapes=[
            pltpu.VMEM((rows, width), jnp.bfloat16),
            pltpu.VMEM((rows, features), jnp.bfloat16),
            pltpu.VMEM(w_glu.shape, jnp.bfloat16),
            pltpu.VMEM(w_branch.shape, jnp.bfloat16),
            pltpu.SemaphoreType.DMA((3,)),
        ],
        compiler_params=pltpu.CompilerParams(vmem_limit_bytes=60 * 1024 * 1024),
        name="glu",
    )(blocks, b_glu.reshape(1, -1), norm_gain.reshape(1, -1), w_glu, w_branch, residual_in)


def place_sums(stream, chunks):
    planes = lax.axis_size("sp")
    rows, features = stream.shape
    size = features // planes
    half = size // 2
    flat = [value for unused, values in chunks for value in values]

    def kernel(stream_ref, *refs):
        at = (lax.axis_index("sp"), lax.axis_index("grp"))
        values, out, total = (list(refs[:-2]), refs[-2], refs[-1])
        total[...] = stream_ref[...]

        def add(value, source, target, length):
            spot = pl.ds(pl.multiple_of(target, LANES), length)
            total[:, spot] += value[:, pl.ds(source, length)].astype(jnp.float32)

        for distances, sums in chunks:
            for ahead in range(len(sums)):
                value, source = (values.pop(0), 0)
                for d in distances:
                    block = (at[0] + (ahead - d + planes)) % planes * size
                    if d == 0:
                        add(value, source, block, size)
                    else:
                        add(value, source, block + at[1] * half, half)
                        add(value, source + half, block + (1 - at[1]) * half, half)
                    source += size
        out[...] = total[...].astype(jnp.bfloat16)

    vmem = pl.BlockSpec(memory_space=pltpu.VMEM)
    return pl.pallas_call(
        kernel,
        in_specs=[vmem] * (1 + len(flat)),
        out_specs=vmem,
        out_shape=jax.ShapeDtypeStruct((rows, features), jnp.bfloat16),
        scratch_shapes=[pltpu.VMEM((rows, features), jnp.float32)],
        compiler_params=pltpu.CompilerParams(vmem_limit_bytes=8 * 1024 * 1024),
        name="place_sums",
    )(stream, *flat)


def feed_forward(stream, normed, wides, talls, units):
    planes = lax.axis_size("sp")
    tokens = [normed]
    for d in range(1, planes):
        tokens.append(hop(normed, "sp", d))
    others = []
    for d in range(planes):
        others.append(swap(tokens[d], "tp", 2))
    own_hidden, tokens = gate_up(tokens + others, wides, 0, units)
    other_hidden = gate_up(tokens, wides, 1, units)[0]
    order = list(range(1, planes))
    chunks = []
    for distances in ([0, 1], order[1:]):
        kept, sent = down((own_hidden, other_hidden), talls, distances)
        sent = swap(sent, "tp", 2)
        values = list(add_sums(kept, sent, planes))
        for d in range(1, planes):
            values[d] = hop(values[d], "sp", -d)
        chunks.append((distances, values))
    return place_sums(stream, chunks)


def per_device(
    ssm_input,
    residual_in,
    log_step,
    decay_real,
    freq,
    in_real,
    in_imag,
    out_real,
    out_imag,
    skip,
    w_glu,
    b_glu,
    w_branch,
    norm_gain,
    w_gate,
    w_up,
    w_down,
):
    tok_rows, width_local = ssm_input.shape
    group_count = log_step.shape[0]
    group_size = in_real.shape[2]
    tp_count = lax.axis_size("tp")
    tp_index = lax.axis_index("tp")
    own_rows = tok_rows // tp_count
    if can_reshard(tok_rows, group_count, in_real.shape, w_gate, w_down):
        wides, talls = reshard(w_gate, w_up, w_down)
        mixer_out = mixer(
            ssm_input, log_step, decay_real, freq, in_real, in_imag, out_real, out_imag, skip
        )
        blocks = lax.all_to_all(
            mixer_out.reshape(tp_count, own_rows, width_local), "tp", split_axis=0, concat_axis=0, tiled=True
        )
        stream, normed = gated_branch(blocks, w_glu, b_glu, w_branch, residual_in, norm_gain)
        return feed_forward(stream, normed, wides, talls, w_gate.shape[1])
    step_size, abar_re, _, bbar_re, bbar_im = discretize(
        log_step, decay_real, freq, in_real, in_imag
    )
    pow_re, pow_im = powers(decay_real, freq, step_size, tok_rows)
    inputs = ssm_input.astype(jnp.float32).reshape(tok_rows, group_count, group_size)
    local_re, local_im = local_states(inputs, decay_real, freq, step_size, bbar_re, bbar_im)
    identity = (
        jnp.ones_like(abar_re),
        jnp.zeros_like(abar_re),
        jnp.zeros_like(abar_re),
        jnp.zeros_like(abar_re),
    )
    carried = prefix((pow_re[-1], pow_im[-1], local_re[-1], local_im[-1]), "sp", compose, identity)
    state_re = local_re + pow_re * carried[2][None] - pow_im * carried[3][None]
    state_im = local_im + pow_re * carried[3][None] + pow_im * carried[2][None]
    mixer_out = readout(
        state_re, state_im, out_real, out_imag, skip.reshape(group_count, group_size), inputs
    )
    mixer_rows = lax.all_to_all(mixer_out, "tp", split_axis=0, concat_axis=1, tiled=True)
    glu_pre = jnp.dot(mixer_rows, w_glu, preferred_element_type=jnp.float32) + b_glu
    gated = (mixer_rows.astype(jnp.float32) * jax.nn.sigmoid(glu_pre)).astype(jnp.bfloat16)
    residual_own = lax.dynamic_slice_in_dim(residual_in, tp_index * own_rows, own_rows, 0)
    stream = residual_own.astype(jnp.float32) + jnp.dot(
        gated, w_branch, preferred_element_type=jnp.float32
    )
    normed = row_norm(stream, norm_gain)
    normed_all = lax.all_gather(normed, "tp", axis=0, tiled=True)
    gate_sum = jnp.dot(
        normed_all,
        lax.all_gather(w_gate, "sp", axis=0, tiled=True),
        preferred_element_type=jnp.float32,
    )
    up_sum = jnp.dot(
        normed_all,
        lax.all_gather(w_up, "sp", axis=0, tiled=True),
        preferred_element_type=jnp.float32,
    )
    hidden = (jax.nn.silu(gate_sum) * up_sum).astype(jnp.bfloat16)
    down_whole = lax.all_gather(w_down, "sp", axis=1, tiled=True)
    summed = lax.psum_scatter(
        jnp.dot(hidden, down_whole, preferred_element_type=jnp.float32).astype(jnp.bfloat16),
        "tp",
        scatter_dimension=0,
        tiled=True,
    ).astype(jnp.float32)
    return (stream + summed).astype(jnp.bfloat16)


def solution(mesh):
    placed = (
        P(("grp", "sp"), "tp"),
        P(("grp", "sp"), None),
        P("tp"),
        P("tp", None),
        P("tp", None),
        P("tp", None, None),
        P("tp", None, None),
        P("tp", None, None),
        P("tp", None, None),
        P("tp"),
        P(),
        P(),
        P(),
        P(),
        P("sp", "tp"),
        P("sp", "tp"),
        P("tp", "sp"),
    )

    return jax.shard_map(
        per_device,
        mesh=mesh,
        in_specs=placed,
        out_specs=P(("grp", "sp", "tp"), None),
        check_vma=False,
    )
```

profile of v0, /device:TPU:0, one launch (start us, length us, event | category | flops | bytes accessed | tf_op | source)
XLA Modules:
  0.0 171.4 jit_solution(14209880792606950833)
XLA Ops:
  4.7 3.5 %local_scan.1 = (f32[128,1024]{1,0:T(8,128)S(1)}, f32[128,1024]{1,0:T(8,128)S(1)}, f32[2,1024]{1,0:T(2,128)S(1)}, f32[2,1024]{1,0:T(2,128)S(1)}) custom-call(f32[16]{0:T(128)S(1)} %copy-done.12, bf16[128,256]{1,0:T(8,128)(2,1)S(1)} %copy-done.2, f32[16,64]{1,0:T(8,128)S(1)} %copy-done.9, f32[16,64]{1,0:T(8,128)S(1)} %copy-done.10, f32[256,64]{1,0:T(8,128)S(1)} %bitcast.15, ...), custom_call_target="tpu_custom_call" | custom-call | tf_op jit(solution)/shard_map/local_scan/pallas_call | solution.py:242
  8.2 5.0 %collective-permute-start = (f32[2,1024]{1,0:T(2,128)S(1)}, f32[2,1024]{1,0:T(2,128)S(1)}, u32[]{:S(2)}, u32[]{:S(2)}) collective-permute-start(f32[2,1024]{1,0:T(2,128)S(1)} %get-tuple-element.37), channel_id=1, source_target_pairs={{0,4},{4,8},{8,12},{1,5},{5,9},{9,13},{2,6},{6,10},{10,14},{3,7},{... | collective-permute-start | bytes 24584 | tf_op jit(solution)/shard_map/ppermute | solution.py:336
  13.2 4.5 %collective-permute-start.1 = (f32[2,1024]{1,0:T(2,128)S(1)}, f32[2,1024]{1,0:T(2,128)S(1)}, u32[]{:S(2)}, u32[]{:S(2)}) collective-permute-start(f32[2,1024]{1,0:T(2,128)S(1)} %get-tuple-element.37), channel_id=1, source_target_pairs={{0,8},{4,12},{1,9},{5,13},{2,10},{6,14},{3,11},{7,15},{16,24},{20,... | collective-permute-start | bytes 24584 | tf_op jit(solution)/shard_map/ppermute | solution.py:336
  24.3 7.2 %all_to_all.5.block = bf16[4,32,256]{2,1,0:T(8,128)(2,1)} all-to-all(bf16[4,32,256]{2,1,0:T(8,128)(2,1)S(1)} %bitcast.12), channel_id=1, replica_groups=mesh['grp'=2,'sp'=4,'tp'=4] {'tp'}, dimensions={0} | all-to-all | bytes 131072 | tf_op jit(solution)/shard_map/all_to_all | solution.py:669
  31.5 5.3 %glu.1 = (f32[32,2048]{1,0:T(8,128)}, bf16[32,2048]{1,0:T(8,128)(2,1)}) custom-call(bf16[4,32,256]{2,1,0:T(8,128)(2,1)} %all_to_all.5.block, f32[1,1024]{1,0:T(1,128)} %bitcast.19, f32[1,2048]{1,0:T(1,128)} %bitcast.18, bf16[1024,1024]{1,0:T(8,128)(2,1)} %glu_hbm.1, bf16[1024,2048]{1,0:T(8,128)(2,1)} %branch_hbm.1, bf16[128,2048]{1,0:T(8,128)(2,1)} %residual.1), custom_call_target="tpu_custom_call" | custom-call | tf_op jit(solution)/shard_map/glu/pallas_call | solution.py:556
  36.9 4.6 %collective-permute-start.4 = (bf16[32,2048]{1,0:T(8,128)(2,1)}, bf16[32,2048]{1,0:T(8,128)(2,1)S(1)}, u32[]{:S(2)}, u32[]{:S(2)}) collective-permute-start(bf16[32,2048]{1,0:T(8,128)(2,1)} %get-tuple-element.39.refs_0_), channel_id=1, source_target_pairs={{0,8},{4,12},{8,0},{12,4},{1,9},{5,13},{9,1},{13,5},{2,10},{6,14},... | collective-permute-start | bytes 393224 | tf_op jit(solution)/shard_map/ppermute | solution.py:153
  41.8 2.0 %shard_map.163 = (bf16[256,768]{1,0:T(8,128)(2,1)}, bf16[256,384]{1,0:T(8,128)(2,1)}) custom-call(bf16[512,1408]{1,0:T(8,128)(2,1)} %gate.5, bf16[512,1408]{1,0:T(8,128)(2,1)} %up.5, bf16[1408,512]{1,0:T(8,128)(2,1)} %down.5), custom_call_target="tpu_custom_call" | custom-call | tf_op jit(solution)/shard_map/pallas_call | solution.py:385
  48.8 2.7 %shard_map.165 = (bf16[512,768]{1,0:T(8,128)(2,1)}, bf16[384,256]{1,0:T(8,128)(2,1)}, bf16[384,256]{1,0:T(8,128)(2,1)}, bf16[384,256]{1,0:T(8,128)(2,1)}, bf16[384,512]{1,0:T(8,128)(2,1)}) custom-call(bf16[512,1408]{1,0:T(8,128)(2,1)} %gate.5, bf16[512,1408]{1,0:T(8,128)(2,1)} %up.5, bf16[1408,512]{1,0:T(8,128)(2,1)} %down.5), custom_call_target="tpu_custom_call" | custom-call | tf_op jit(solution)/shard_map/pallas_call | solution.py:385
  51.6 7.5 %collective-permute-start.28 = (bf16[384,256]{1,0:T(8,128)(2,1)}, bf16[384,256]{1,0:T(8,128)(2,1)S(1)}, u32[]{:S(2)}, u32[]{:S(2)}) collective-permute-start(bf16[384,256]{1,0:T(8,128)(2,1)} %get-tuple-element.48), channel_id=1, source_target_pairs={{0,4},{4,8},{8,12},{12,0},{1,5},{5,9},{9,13},{13,1},{2,6},{6,10},{... | collective-permute-start | bytes 589832 | tf_op jit(solution)/shard_map/ppermute | solution.py:153
  59.1 3.3 %collective-permute-start.36 = (bf16[384,256]{1,0:T(8,128)(2,1)}, bf16[384,256]{1,0:T(8,128)(2,1)S(1)}, u32[]{:S(2)}, u32[]{:S(2)}) collective-permute-start(bf16[384,256]{1,0:T(8,128)(2,1)} %get-tuple-element.55), channel_id=1, source_target_pairs={{0,8},{4,12},{8,0},{12,4},{1,9},{5,13},{9,1},{13,5},{2,10},{6,14},... | collective-permute-start | bytes 589832 | tf_op jit(solution)/shard_map/ppermute | solution.py:153
  64.4 3.4 %collective-permute-done.28.refs_2_ = bf16[384,256]{1,0:T(8,128)(2,1)S(1)} collective-permute-done((bf16[384,256]{1,0:T(8,128)(2,1)}, bf16[384,256]{1,0:T(8,128)(2,1)S(1)}, u32[]{:S(2)}, u32[]{:S(2)}) %collective-permute-start.28) | collective-permute-done | bytes 196640 | tf_op jit(solution)/shard_map/ppermute | solution.py:153
  68.0 8.3 %collective-permute-done.36.refs_0_ = bf16[384,256]{1,0:T(8,128)(2,1)S(1)} collective-permute-done((bf16[384,256]{1,0:T(8,128)(2,1)}, bf16[384,256]{1,0:T(8,128)(2,1)S(1)}, u32[]{:S(2)}, u32[]{:S(2)}) %collective-permute-start.36) | collective-permute-done | bytes 196640 | tf_op jit(solution)/shard_map/ppermute | solution.py:153
  79.8 2.8 %collective-permute-done.8.refs_6_ = bf16[32,2048]{1,0:T(8,128)(2,1)S(1)} collective-permute-done((bf16[32,2048]{1,0:T(8,128)(2,1)S(1)}, bf16[32,2048]{1,0:T(8,128)(2,1)S(1)}, u32[]{:S(2)}, u32[]{:S(2)}) %collective-permute-start.8) | collective-permute-done | bytes 131104 | tf_op jit(solution)/shard_map/ppermute | solution.py:157
  86.3 18.1 %collective-permute-done.14.refs_12_ = bf16[256,768]{1,0:T(8,128)(2,1)S(1)} collective-permute-done((bf16[256,768]{1,0:T(8,128)(2,1)S(1)}, bf16[256,768]{1,0:T(8,128)(2,1)S(1)}, u32[]{:S(2)}, u32[]{:S(2)}) %collective-permute-start.14) | collective-permute-done | bytes 393248 | tf_op jit(solution)/shard_map/ppermute | solution.py:153
  108.6 3.6 %collective-permute-done.30.refs_4_ = bf16[384,256]{1,0:T(8,128)(2,1)S(1)} collective-permute-done((bf16[384,256]{1,0:T(8,128)(2,1)S(1)}, bf16[384,256]{1,0:T(8,128)(2,1)S(1)}, u32[]{:S(2)}, u32[]{:S(2)}) %collective-permute-start.30) | collective-permute-done | bytes 196640 | tf_op jit(solution)/shard_map/ppermute | solution.py:157
  113.7 2.7 %collective-permute-done.38.refs_2_ = bf16[384,256]{1,0:T(8,128)(2,1)S(1)} collective-permute-done((bf16[384,256]{1,0:T(8,128)(2,1)S(1)}, bf16[384,256]{1,0:T(8,128)(2,1)S(1)}, u32[]{:S(2)}, u32[]{:S(2)}) %collective-permute-start.38) | collective-permute-done | bytes 196640 | tf_op jit(solution)/shard_map/ppermute | solution.py:157
  116.4 4.2 %collective-permute-done.42.refs_6_ = bf16[384,256]{1,0:T(8,128)(2,1)S(1)} collective-permute-done((bf16[384,256]{1,0:T(8,128)(2,1)S(1)}, bf16[384,256]{1,0:T(8,128)(2,1)S(1)}, u32[]{:S(2)}, u32[]{:S(2)}) %collective-permute-start.42) | collective-permute-done | bytes 196640 | tf_op jit(solution)/shard_map/ppermute | solution.py:157
  122.2 6.8 %collective-permute-done.11.refs_9_ = bf16[256,768]{1,0:T(8,128)(2,1)S(1)} collective-permute-done((bf16[256,768]{1,0:T(8,128)(2,1)S(1)}, bf16[256,768]{1,0:T(8,128)(2,1)S(1)}, u32[]{:S(2)}, u32[]{:S(2)}) %collective-permute-start.11) | collective-permute-done | bytes 393248 | tf_op jit(solution)/shard_map/ppermute | solution.py:157
  129.1 8.0 %collective-permute-done.15.refs_13_ = bf16[256,768]{1,0:T(8,128)(2,1)S(1)} collective-permute-done((bf16[256,768]{1,0:T(8,128)(2,1)S(1)}, bf16[256,768]{1,0:T(8,128)(2,1)S(1)}, u32[]{:S(2)}, u32[]{:S(2)}) %collective-permute-start.15) | collective-permute-done | bytes 393248 | tf_op jit(solution)/shard_map/ppermute | solution.py:157
  140.0 3.6 %shard_map.166 = (bf16[256,384]{1,0:T(8,128)(2,1)S(1)}, bf16[256,2048]{1,0:T(8,128)(2,1)S(1)}) custom-call(bf16[32,2048]{1,0:T(8,128)(2,1)S(1)} %copy-done.6, bf16[32,2048]{1,0:T(8,128)(2,1)S(1)} %collective-permute-done.3.refs_1_, bf16[32,2048]{1,0:T(8,128)(2,1)S(1)} %collective-permute-done.4.refs_2_, bf16[32,2048]{1,0:T(8,128)(2,1)S(1)} %collective-permute-done.5.refs_3_, ...), custom_call_target="tpu_custom_call" | custom-call | tf_op jit(solution)/shard_map/pallas_call | solution.py:457
  149.8 6.0 %collective-permute-done.32.b = bf16[128,1024]{1,0:T(8,128)(2,1)S(1)} collective-permute-done((bf16[128,1024]{1,0:T(8,128)(2,1)S(1)}, bf16[128,1024]{1,0:T(8,128)(2,1)S(1)}, u32[]{:S(2)}, u32[]{:S(2)}) %collective-permute-start.32) | collective-permute-done | bytes 262176 | tf_op jit(solution)/shard_map/ppermute | solution.py:157
  156.0 2.9 %collective-permute-start.34 = (bf16[32,1024]{1,0:T(8,128)(2,1)S(1)}, bf16[32,1024]{1,0:T(8,128)(2,1)S(1)}, u32[]{:S(2)}, u32[]{:S(2)}) collective-permute-start(bf16[32,1024]{1,0:T(8,128)(2,1)S(1)} %get-tuple-element.53), channel_id=1, source_target_pairs={{0,8},{4,12},{8,0},{12,4},{1,9},{5,13},{9,1},{13,5},{2,10},{6,14},... | collective-permute-start | bytes 196616 | tf_op jit(solution)/shard_map/ppermute | solution.py:153
  158.8 2.0 %collective-permute-done.44.b = bf16[128,1024]{1,0:T(8,128)(2,1)S(1)} collective-permute-done((bf16[128,1024]{1,0:T(8,128)(2,1)S(1)}, bf16[128,1024]{1,0:T(8,128)(2,1)S(1)}, u32[]{:S(2)}, u32[]{:S(2)}) %collective-permute-start.44) | collective-permute-done | bytes 262176 | tf_op jit(solution)/shard_map/ppermute | solution.py:157
  165.9 4.7 %collective-permute-done.46.refs_6_ = bf16[32,1024]{1,0:T(8,128)(2,1)S(1)} collective-permute-done((bf16[32,1024]{1,0:T(8,128)(2,1)S(1)}, bf16[32,1024]{1,0:T(8,128)(2,1)S(1)}, u32[]{:S(2)}, u32[]{:S(2)}) %collective-permute-start.46) | collective-permute-done | bytes 65568 | tf_op jit(solution)/shard_map/ppermute | solution.py:153
  (116 shorter events, 48.5 us)
Async XLA Ops:
  8.2 10.8 %collective-permute-start = (f32[2,1024]{1,0:T(2,128)S(1)}, f32[2,1024]{1,0:T(2,128)S(1)}, u32[]{:S(2)}, u32[]{:S(2)}) collective-permute-start(f32[2,1024]{1,0:T(2,128)S(1)} %get-tuple-element.37), channel_id=1, source_target_pairs={{0,4},{4,8},{8,12},{1,5},{5,9},{9,13},{2,6},{6,10},{10,14},{3,7},{... | collective-permute-start | bytes 24584 | tf_op jit(solution)/shard_map/ppermute | solution.py:336
  36.9 14.7 %collective-permute-start.4 = (bf16[32,2048]{1,0:T(8,128)(2,1)}, bf16[32,2048]{1,0:T(8,128)(2,1)S(1)}, u32[]{:S(2)}, u32[]{:S(2)}) collective-permute-start(bf16[32,2048]{1,0:T(8,128)(2,1)} %get-tuple-element.39.refs_0_), channel_id=1, source_target_pairs={{0,8},{4,12},{8,0},{12,4},{1,9},{5,13},{9,1},{13,5},{2,10},{6,14},... | collective-permute-start | bytes 393224 | tf_op jit(solution)/shard_map/ppermute | solution.py:153
  41.5 17.5 %collective-permute-start.5 = (bf16[32,2048]{1,0:T(8,128)(2,1)}, bf16[32,2048]{1,0:T(8,128)(2,1)S(1)}, u32[]{:S(2)}, u32[]{:S(2)}) collective-permute-start(bf16[32,2048]{1,0:T(8,128)(2,1)} %get-tuple-element.39.refs_0_), channel_id=1, source_target_pairs={{0,12},{4,0},{8,4},{12,8},{1,13},{5,1},{9,5},{13,9},{2,14},{6,2},{... | collective-permute-start | bytes 393224 | tf_op jit(solution)/shard_map/ppermute | solution.py:153
  41.7 20.7 %collective-permute-start.6 = (bf16[32,2048]{1,0:T(8,128)(2,1)}, bf16[32,2048]{1,0:T(8,128)(2,1)S(1)}, u32[]{:S(2)}, u32[]{:S(2)}) collective-permute-start(bf16[32,2048]{1,0:T(8,128)(2,1)} %get-tuple-element.39.refs_0_), channel_id=1, source_target_pairs={{0,2},{1,3},{2,0},{3,1},{4,6},{5,7},{6,4},{7,5},{8,10},{9,11},{10,... | collective-permute-start | bytes 393224 | tf_op jit(solution)/shard_map/ppermute | solution.py:157
  43.9 18.5 %collective-permute-start.12 = (bf16[256,384]{1,0:T(8,128)(2,1)}, bf16[256,384]{1,0:T(8,128)(2,1)S(1)}, u32[]{:S(2)}, u32[]{:S(2)}) collective-permute-start(bf16[256,384]{1,0:T(8,128)(2,1)} %get-tuple-element.41), channel_id=1, source_target_pairs={{0,12},{4,0},{8,4},{12,8},{1,13},{5,1},{9,5},{13,9},{2,14},{6,2},{... | collective-permute-start | bytes 589832 | tf_op jit(solution)/shard_map/ppermute | solution.py:153
  47.3 17.1 %collective-permute-start.16 = (bf16[256,384]{1,0:T(8,128)(2,1)}, bf16[256,384]{1,0:T(8,128)(2,1)S(1)}, u32[]{:S(2)}, u32[]{:S(2)}) collective-permute-start(bf16[256,384]{1,0:T(8,128)(2,1)} %get-tuple-element.43), channel_id=1, source_target_pairs={{0,12},{4,0},{8,4},{12,8},{1,13},{5,1},{9,5},{13,9},{2,14},{6,2},{... | collective-permute-start | bytes 589832 | tf_op jit(solution)/shard_map/ppermute | solution.py:153
  51.6 16.3 %collective-permute-start.28 = (bf16[384,256]{1,0:T(8,128)(2,1)}, bf16[384,256]{1,0:T(8,128)(2,1)S(1)}, u32[]{:S(2)}, u32[]{:S(2)}) collective-permute-start(bf16[384,256]{1,0:T(8,128)(2,1)} %get-tuple-element.48), channel_id=1, source_target_pairs={{0,4},{4,8},{8,12},{12,0},{1,5},{5,9},{9,13},{13,1},{2,6},{6,10},{... | collective-permute-start | bytes 589832 | tf_op jit(solution)/shard_map/ppermute | solution.py:153
  59.1 17.2 %collective-permute-start.36 = (bf16[384,256]{1,0:T(8,128)(2,1)}, bf16[384,256]{1,0:T(8,128)(2,1)S(1)}, u32[]{:S(2)}, u32[]{:S(2)}) collective-permute-start(bf16[384,256]{1,0:T(8,128)(2,1)} %get-tuple-element.55), channel_id=1, source_target_pairs={{0,8},{4,12},{8,0},{12,4},{1,9},{5,13},{9,1},{13,5},{2,10},{6,14},... | collective-permute-start | bytes 589832 | tf_op jit(solution)/shard_map/ppermute | solution.py:153
  62.3 14.1 %collective-permute-start.40 = (bf16[384,256]{1,0:T(8,128)(2,1)}, bf16[384,256]{1,0:T(8,128)(2,1)S(1)}, u32[]{:S(2)}, u32[]{:S(2)}) collective-permute-start(bf16[384,256]{1,0:T(8,128)(2,1)} %get-tuple-element.56), channel_id=1, source_target_pairs={{0,12},{4,0},{8,4},{12,8},{1,13},{5,1},{9,5},{13,9},{2,14},{6,2},{... | collective-permute-start | bytes 589832 | tf_op jit(solution)/shard_map/ppermute | solution.py:153
  62.4 23.4 %collective-permute-start.10 = (bf16[256,768]{1,0:T(8,128)(2,1)S(1)}, bf16[256,768]{1,0:T(8,128)(2,1)S(1)}, u32[]{:S(2)}, u32[]{:S(2)}) collective-permute-start(bf16[256,768]{1,0:T(8,128)(2,1)S(1)} %copy-done.14), channel_id=1, source_target_pairs={{0,4},{4,8},{8,12},{12,0},{1,5},{5,9},{9,13},{13,1},{2,6},{6,10},{... | collective-permute-start | bytes 1179656 | tf_op jit(solution)/shard_map/ppermute | solution.py:153
  64.4 40.0 %collective-permute-start.14 = (bf16[256,768]{1,0:T(8,128)(2,1)S(1)}, bf16[256,768]{1,0:T(8,128)(2,1)S(1)}, u32[]{:S(2)}, u32[]{:S(2)}) collective-permute-start(bf16[256,768]{1,0:T(8,128)(2,1)S(1)} %copy-done.13), channel_id=1, source_target_pairs={{0,8},{4,12},{8,0},{12,4},{1,9},{5,13},{9,1},{13,5},{2,10},{6,14},... | collective-permute-start | bytes 1179656 | tf_op jit(solution)/shard_map/ppermute | solution.py:153
  67.8 10.5 %collective-permute-start.7 = (bf16[32,2048]{1,0:T(8,128)(2,1)S(1)}, bf16[32,2048]{1,0:T(8,128)(2,1)S(1)}, u32[]{:S(2)}, u32[]{:S(2)}) collective-permute-start(bf16[32,2048]{1,0:T(8,128)(2,1)S(1)} %collective-permute-done.3.refs_1_), channel_id=1, source_target_pairs={{0,2},{1,3},{2,0},{3,1},{4,6},{5,7},{6,4},{7,5},{8,10},{9,11},{10,... | collective-permute-start | bytes 393224 | tf_op jit(solution)/shard_map/ppermute | solution.py:157
  82.6 25.4 %collective-permute-start.27 = (bf16[384,512]{1,0:T(8,128)(2,1)}, bf16[384,512]{1,0:T(8,128)(2,1)S(1)}, u32[]{:S(2)}, u32[]{:S(2)}) collective-permute-start(bf16[384,512]{1,0:T(8,128)(2,1)} %get-tuple-element.47.refs_0_), channel_id=1, source_target_pairs={{0,1},{1,0},{2,3},{3,2},{4,5},{5,4},{6,7},{7,6},{8,9},{9,8},{10,11... | collective-permute-start | bytes 1179656 | tf_op jit(solution)/shard_map/ppermute | solution.py:157
  84.2 20.2 %collective-permute-start.17 = (bf16[256,384]{1,0:T(8,128)(2,1)S(1)}, bf16[256,384]{1,0:T(8,128)(2,1)S(1)}, u32[]{:S(2)}, u32[]{:S(2)}) collective-permute-start(bf16[256,384]{1,0:T(8,128)(2,1)S(1)} %collective-permute-done.16.refs_14_), channel_id=1, source_target_pairs={{0,16},{16,0},{1,17},{17,1},{2,18},{18,2},{3,19},{19,3},{4,20},{20... | collective-permute-start | bytes 589832 | tf_op jit(solution)/shard_map/ppermute | solution.py:157
  85.8 20.2 %collective-permute-start.20 = (bf16[256,384]{1,0:T(8,128)(2,1)S(1)}, bf16[256,384]{1,0:T(8,128)(2,1)S(1)}, u32[]{:S(2)}, u32[]{:S(2)}) collective-permute-start(bf16[256,384]{1,0:T(8,128)(2,1)S(1)} %collective-permute-done.12.refs_10_), channel_id=1, source_target_pairs={{0,1},{1,0},{2,3},{3,2},{4,5},{5,4},{6,7},{7,6},{8,9},{9,8},{10,11... | collective-permute-start | bytes 589832 | tf_op jit(solution)/shard_map/ppermute | solution.py:157
  85.8 20.7 %collective-permute-start.24 = (bf16[256,384]{1,0:T(8,128)(2,1)S(1)}, bf16[256,384]{1,0:T(8,128)(2,1)S(1)}, u32[]{:S(2)}, u32[]{:S(2)}) collective-permute-start(bf16[256,384]{1,0:T(8,128)(2,1)S(1)} %collective-permute-done.16.refs_14_), channel_id=1, source_target_pairs={{0,1},{1,0},{2,3},{3,2},{4,5},{5,4},{6,7},{7,6},{8,9},{9,8},{10,11... | collective-permute-start | bytes 589832 | tf_op jit(solution)/shard_map/ppermute | solution.py:157
  106.0 10.5 %collective-permute-start.38 = (bf16[384,256]{1,0:T(8,128)(2,1)S(1)}, bf16[384,256]{1,0:T(8,128)(2,1)S(1)}, u32[]{:S(2)}, u32[]{:S(2)}) collective-permute-start(bf16[384,256]{1,0:T(8,128)(2,1)S(1)} %collective-permute-done.36.refs_0_), channel_id=1, source_target_pairs={{0,16},{16,0},{1,17},{17,1},{2,18},{18,2},{3,19},{19,3},{4,20},{20... | collective-permute-start | bytes 589832 | tf_op jit(solution)/shard_map/ppermute | solution.py:157
  106.5 14.2 %collective-permute-start.42 = (bf16[384,256]{1,0:T(8,128)(2,1)S(1)}, bf16[384,256]{1,0:T(8,128)(2,1)S(1)}, u32[]{:S(2)}, u32[]{:S(2)}) collective-permute-start(bf16[384,256]{1,0:T(8,128)(2,1)S(1)} %collective-permute-done.40.refs_4_), channel_id=1, source_target_pairs={{0,16},{16,0},{1,17},{17,1},{2,18},{18,2},{3,19},{19,3},{4,20},{20... | collective-permute-start | bytes 589832 | tf_op jit(solution)/shard_map/ppermute | solution.py:157
  108.0 29.6 %collective-permute-start.26 = (bf16[512,768]{1,0:T(8,128)(2,1)}, bf16[512,768]{1,0:T(8,128)(2,1)S(1)}, u32[]{:S(2)}, u32[]{:S(2)}) collective-permute-start(bf16[512,768]{1,0:T(8,128)(2,1)} %get-tuple-element.44.refs_16_), channel_id=1, source_target_pairs={{0,1},{1,0},{2,3},{3,2},{4,5},{5,4},{6,7},{7,6},{8,9},{9,8},{10,11... | collective-permute-start | bytes 2359304 | tf_op jit(solution)/shard_map/ppermute | solution.py:157
  108.0 21.1 %collective-permute-start.11 = (bf16[256,768]{1,0:T(8,128)(2,1)S(1)}, bf16[256,768]{1,0:T(8,128)(2,1)S(1)}, u32[]{:S(2)}, u32[]{:S(2)}) collective-permute-start(bf16[256,768]{1,0:T(8,128)(2,1)S(1)} %collective-permute-done.10.refs_8_), channel_id=1, source_target_pairs={{0,16},{16,0},{1,17},{17,1},{2,18},{18,2},{3,19},{19,3},{4,20},{20... | collective-permute-start | bytes 1179656 | tf_op jit(solution)/shard_map/ppermute | solution.py:157
  112.2 24.8 %collective-permute-start.15 = (bf16[256,768]{1,0:T(8,128)(2,1)S(1)}, bf16[256,768]{1,0:T(8,128)(2,1)S(1)}, u32[]{:S(2)}, u32[]{:S(2)}) collective-permute-start(bf16[256,768]{1,0:T(8,128)(2,1)S(1)} %collective-permute-done.14.refs_12_), channel_id=1, source_target_pairs={{0,16},{16,0},{1,17},{17,1},{2,18},{18,2},{3,19},{19,3},{4,20},{20... | collective-permute-start | bytes 1179656 | tf_op jit(solution)/shard_map/ppermute | solution.py:157
  120.6 16.4 %collective-permute-start.18 = (bf16[256,768]{1,0:T(8,128)(2,1)S(1)}, bf16[256,768]{1,0:T(8,128)(2,1)S(1)}, u32[]{:S(2)}, u32[]{:S(2)}) collective-permute-start(bf16[256,768]{1,0:T(8,128)(2,1)S(1)} %collective-permute-done.10.refs_8_), channel_id=1, source_target_pairs={{0,1},{1,0},{2,3},{3,2},{4,5},{5,4},{6,7},{7,6},{8,9},{9,8},{10,11... | collective-permute-start | bytes 1179656 | tf_op jit(solution)/shard_map/ppermute | solution.py:157
  122.1 15.5 %collective-permute-start.22 = (bf16[256,768]{1,0:T(8,128)(2,1)S(1)}, bf16[256,768]{1,0:T(8,128)(2,1)S(1)}, u32[]{:S(2)}, u32[]{:S(2)}) collective-permute-start(bf16[256,768]{1,0:T(8,128)(2,1)S(1)} %collective-permute-done.14.refs_12_), channel_id=1, source_target_pairs={{0,1},{1,0},{2,3},{3,2},{4,5},{5,4},{6,7},{7,6},{8,9},{9,8},{10,11... | collective-permute-start | bytes 1179656 | tf_op jit(solution)/shard_map/ppermute | solution.py:157
  147.9 13.0 %collective-permute-start.44 = (bf16[128,1024]{1,0:T(8,128)(2,1)S(1)}, bf16[128,1024]{1,0:T(8,128)(2,1)S(1)}, u32[]{:S(2)}, u32[]{:S(2)}) collective-permute-start(bf16[128,1024]{1,0:T(8,128)(2,1)S(1)} %get-tuple-element.58), channel_id=1, source_target_pairs={{0,2},{1,3},{2,0},{3,1},{4,6},{5,7},{6,4},{7,5},{8,10},{9,11},{10,... | collective-permute-start | bytes 786440 | tf_op jit(solution)/shard_map/ppermute | solution.py:157
  (39 other events, 321.8 us)
where the time goes:
time: 172 us; the launch traced here: 171 us
  waiting for transfers between devices  77 us (45%)
  starting transfers between devices  53.1 us (31%)
  Pallas kernels  25.5 us (15%)
  local copies, waits for them, and re-layouts  8.34 us (5%)
  blocking collectives  7.16 us (4%)
    ppermute x29, waiting for transfers between devices, swap(): lax.ppermute(value, axis, [(i, i ^ bit) for i in range(lax.axis_size(axis...  39.4 us
    ppermute x16, waiting for transfers between devices, hop(): lax.ppermute(value, axis, [(i, (i + distance) % count) for i in range(cou...  36.3 us
    ppermute x16, starting transfers between devices, hop(): lax.ppermute(value, axis, [(i, (i + distance) % count) for i in range(cou...  26.7 us
    ppermute x29, starting transfers between devices, swap(): lax.ppermute(value, axis, [(i, i ^ bit) for i in range(lax.axis_size(axis...  15.6 us
    ppermute x3, starting transfers between devices, mixer(): lax.ppermute(end, 'sp', [(i, i + d) for i in range(planes - d)])  10.7 us
    unnamed x30, local copies, waits for them, and re-layouts  8.34 us
    all_to_all x1, blocking collectives, per_device(): lax.all_to_all(mixer_out.reshape(tp_count, own_rows, width_local), 'tp',...  7.16 us
    pallas_call x3, Pallas kernels, cut(): pl.pallas_call(kernel, in_specs=[anywhere] * 3, out_specs=[pl.BlockSpec(m...  6.7 us
  transfers between devices with their start and end apart: 48, of which 18 were waited for; matrix products, arithmetic and copies ran while one was open for 0% of the time, Pallas kernels for 8%

commit v1 on v0

--- a/solution.py
+++ b/solution.py
@@ -436,13 +436,24 @@
         tok_refs, weights = (refs[: len(toks)], refs[len(toks) : len(toks) + len(pieces)])
         out, *outs, wide, sems = refs[len(toks) + len(pieces) :]
         tok = tok_refs[0] if whole else outs[0]
-        copies = [] if whole else [(ref, tok.at[pl.ds(i * rows, rows), :]) for i, ref in enumerate(tok_refs)]
+        moves = [] if whole else [(ref, tok.at[pl.ds(i * rows, rows), :]) for i, ref in enumerate(tok_refs)]
+        later = []
         for (start, col), weight in zip(spots, weights):
             row = pl.ds(pl.multiple_of(start, 16), weight.shape[0])
-            copies.append((weight, wide.at[row, pl.ds(col, weight.shape[1])]))
-        run_copies(copies, sems)
-        sums = jnp.dot(tok[...], wide[...], preferred_element_type=jnp.float32)
-        gate, up = (sums[:, :width], sums[:, width:])
+            for first in range(0, weight.shape[1], width):
+                part_of = weight.at[:, pl.ds(first, width)]
+                target = wide.at[row, pl.ds(col + first, width)]
+                (later if col + first else moves).append((part_of, target))
+        count_first = len(moves)
+        copies = [pltpu.make_async_copy(a, b, sems.at[i]) for i, (a, b) in enumerate(moves + later)]
+        for copy in copies:
+            copy.start()
+        for copy in copies[:count_first]:
+            copy.wait()
+        gate = jnp.dot(tok[...], wide[:, :width], preferred_element_type=jnp.float32)
+        for copy in copies[count_first:]:
+            copy.wait()
+        up = jnp.dot(tok[...], wide[:, width:], preferred_element_type=jnp.float32)
         hidden = gate / (1.0 + jnp.exp(-gate)) * up
         live = lax.broadcasted_iota(jnp.int32, hidden.shape, 1) >= place * width - first_unit(
             place, planes, units
@@ -456,12 +467,12 @@
         shapes.append(jax.ShapeDtypeStruct((count, features), jnp.bfloat16))
     return pl.pallas_call(
         kernel,
-        in_specs=[vmem if whole else anywhere] * len(toks) + [anywhere] * len(pieces),
+        in_specs=[vmem] * len(toks) + [anywhere] * len(pieces),
         out_specs=[vmem] * len(shapes),
         out_shape=shapes,
         scratch_shapes=[
             pltpu.VMEM((features, 2 * width), jnp.bfloat16),
-            pltpu.SemaphoreType.DMA((len(toks) + len(pieces),)),
+            pltpu.SemaphoreType.DMA((len(toks) + 2 * len(pieces),)),
         ],
         compiler_params=pltpu.CompilerParams(vmem_limit_bytes=16 * 1024 * 1024),
     )(*toks, *pieces)
@@ -568,7 +579,7 @@
             pltpu.VMEM(w_branch.shape, jnp.bfloat16),
             pltpu.SemaphoreType.DMA((3,)),
         ],
-        compiler_params=pltpu.CompilerParams(vmem_limit_bytes=60 * 1024 * 1024),
+        compiler_params=pltpu.CompilerParams(vmem_limit_bytes=52 * 1024 * 1024),
         name="glu",
     )(blocks, b_glu.reshape(1, -1), norm_gain.reshape(1, -1), w_glu, w_branch, residual_in)
 

time: 172 us -> 170 us (0.988)
    unnamed x30 -> x32, local copies, waits for them, and re-layouts: 8.34 us -> 8.39 us
where the time goes in v1:
time: 170 us; the launch traced here: 169 us
  waiting for transfers between devices  77 us (45%)
  starting transfers between devices  53 us (31%)
  Pallas kernels  23.8 us (14%)
  local copies, waits for them, and re-layouts  8.39 us (5%)
  blocking collectives  6.68 us (4%)
    ppermute x29, waiting for transfers between devices, swap(): lax.ppermute(value, axis, [(i, i ^ bit) for i in range(lax.axis_size(axis...  39.4 us
    ppermute x16, waiting for transfers between devices, hop(): lax.ppermute(value, axis, [(i, (i + distance) % count) for i in range(cou...  36.2 us
    ppermute x16, starting transfers between devices, hop(): lax.ppermute(value, axis, [(i, (i + distance) % count) for i in range(cou...  26.6 us
    ppermute x29, starting transfers between devices, swap(): lax.ppermute(value, axis, [(i, i ^ bit) for i in range(lax.axis_size(axis...  15.6 us
    ppermute x3, starting transfers between devices, mixer(): lax.ppermute(end, 'sp', [(i, i + d) for i in range(planes - d)])  10.7 us
    unnamed x32, local copies, waits for them, and re-layouts  8.39 us
    all_to_all x1, blocking collectives, per_device(): lax.all_to_all(mixer_out.reshape(tp_count, own_rows, width_local), 'tp',...  6.68 us
    pallas_call x3, Pallas kernels, cut(): pl.pallas_call(kernel, in_specs=[anywhere] * 3, out_specs=[pl.BlockSpec(m...  6.64 us
  transfers between devices with their start and end apart: 48, of which 18 were waited for; matrix products, arithmetic and copies ran while one was open for 0% of the time, Pallas kernels for 8%

profile of v1, /device:TPU:0, one launch (start us, length us, event | category | flops | bytes accessed | tf_op | source)
XLA Modules:
  0.0 169.2 jit_solution(13532874521369603408)
XLA Ops:
  4.8 3.5 %local_scan.1 = (f32[128,1024]{1,0:T(8,128)S(1)}, f32[128,1024]{1,0:T(8,128)S(1)}, f32[2,1024]{1,0:T(2,128)S(1)}, f32[2,1024]{1,0:T(2,128)S(1)}) custom-call(f32[16]{0:T(128)S(1)} %copy-done.13, bf16[128,256]{1,0:T(8,128)(2,1)S(1)} %copy-done.3, f32[16,64]{1,0:T(8,128)S(1)} %copy-done.9, f32[16,64]{1,0:T(8,128)S(1)} %copy-done.10, f32[256,64]{1,0:T(8,128)S(1)} %bitcast.15, ...), custom_call_target="tpu_custom_call" | custom-call | tf_op jit(solution)/shard_map/local_scan/pallas_call | solution.py:242
  8.3 5.0 %collective-permute-start = (f32[2,1024]{1,0:T(2,128)S(1)}, f32[2,1024]{1,0:T(2,128)S(1)}, u32[]{:S(2)}, u32[]{:S(2)}) collective-permute-start(f32[2,1024]{1,0:T(2,128)S(1)} %get-tuple-element.37), channel_id=1, source_target_pairs={{0,4},{4,8},{8,12},{1,5},{5,9},{9,13},{2,6},{6,10},{10,14},{3,7},{... | collective-permute-start | bytes 24584 | tf_op jit(solution)/shard_map/ppermute | solution.py:336
  13.2 4.5 %collective-permute-start.1 = (f32[2,1024]{1,0:T(2,128)S(1)}, f32[2,1024]{1,0:T(2,128)S(1)}, u32[]{:S(2)}, u32[]{:S(2)}) collective-permute-start(f32[2,1024]{1,0:T(2,128)S(1)} %get-tuple-element.37), channel_id=1, source_target_pairs={{0,8},{4,12},{1,9},{5,13},{2,10},{6,14},{3,11},{7,15},{16,24},{20,... | collective-permute-start | bytes 24584 | tf_op jit(solution)/shard_map/ppermute | solution.py:336
  24.4 6.7 %all_to_all.5.block = bf16[4,32,256]{2,1,0:T(8,128)(2,1)S(1)} all-to-all(bf16[4,32,256]{2,1,0:T(8,128)(2,1)S(1)} %bitcast.12), channel_id=1, replica_groups=mesh['grp'=2,'sp'=4,'tp'=4] {'tp'}, dimensions={0} | all-to-all | bytes 131072 | tf_op jit(solution)/shard_map/all_to_all | solution.py:680
  31.1 3.8 %glu.1 = (f32[32,2048]{1,0:T(8,128)S(1)}, bf16[32,2048]{1,0:T(8,128)(2,1)S(1)}) custom-call(bf16[4,32,256]{2,1,0:T(8,128)(2,1)S(1)} %all_to_all.5.block, f32[1,1024]{1,0:T(1,128)S(1)} %bitcast.18, f32[1,2048]{1,0:T(1,128)S(1)} %bitcast.17, bf16[1024,1024]{1,0:T(8,128)(2,1)} %glu_hbm.1, bf16[1024,2048]{1,0:T(8,128)(2,1)} %branch_hbm.1, ...), custom_call_target="tpu_custom_call" | custom-call | tf_op jit(solution)/shard_map/glu/pallas_call | solution.py:567
  35.0 4.6 %collective-permute-start.4 = (bf16[32,2048]{1,0:T(8,128)(2,1)S(1)}, bf16[32,2048]{1,0:T(8,128)(2,1)S(1)}, u32[]{:S(2)}, u32[]{:S(2)}) collective-permute-start(bf16[32,2048]{1,0:T(8,128)(2,1)S(1)} %get-tuple-element.39.refs_0_), channel_id=1, source_target_pairs={{0,8},{4,12},{8,0},{12,4},{1,9},{5,13},{9,1},{13,5},{2,10},{6,14},... | collective-permute-start | bytes 393224 | tf_op jit(solution)/shard_map/ppermute | solution.py:153
  46.9 2.7 %shard_map.165 = (bf16[512,768]{1,0:T(8,128)(2,1)}, bf16[384,256]{1,0:T(8,128)(2,1)}, bf16[384,256]{1,0:T(8,128)(2,1)}, bf16[384,256]{1,0:T(8,128)(2,1)}, bf16[384,512]{1,0:T(8,128)(2,1)}) custom-call(bf16[512,1408]{1,0:T(8,128)(2,1)} %gate.5, bf16[512,1408]{1,0:T(8,128)(2,1)} %up.5, bf16[1408,512]{1,0:T(8,128)(2,1)} %down.5), custom_call_target="tpu_custom_call" | custom-call | tf_op jit(solution)/shard_map/pallas_call | solution.py:385
  49.6 7.2 %collective-permute-start.28 = (bf16[384,256]{1,0:T(8,128)(2,1)}, bf16[384,256]{1,0:T(8,128)(2,1)S(1)}, u32[]{:S(2)}, u32[]{:S(2)}) collective-permute-start(bf16[384,256]{1,0:T(8,128)(2,1)} %get-tuple-element.48), channel_id=1, source_target_pairs={{0,4},{4,8},{8,12},{12,0},{1,5},{5,9},{9,13},{13,1},{2,6},{6,10},{... | collective-permute-start | bytes 589832 | tf_op jit(solution)/shard_map/ppermute | solution.py:153
  56.8 3.4 %collective-permute-start.36 = (bf16[384,256]{1,0:T(8,128)(2,1)}, bf16[384,256]{1,0:T(8,128)(2,1)S(1)}, u32[]{:S(2)}, u32[]{:S(2)}) collective-permute-start(bf16[384,256]{1,0:T(8,128)(2,1)} %get-tuple-element.55), channel_id=1, source_target_pairs={{0,8},{4,12},{8,0},{12,4},{1,9},{5,13},{9,1},{13,5},{2,10},{6,14},... | collective-permute-start | bytes 589832 | tf_op jit(solution)/shard_map/ppermute | solution.py:153
  60.2 2.0 %collective-permute-start.10 = (bf16[256,768]{1,0:T(8,128)(2,1)S(1)}, bf16[256,768]{1,0:T(8,128)(2,1)S(1)}, u32[]{:S(2)}, u32[]{:S(2)}) collective-permute-start(bf16[256,768]{1,0:T(8,128)(2,1)S(1)} %copy-done.15), channel_id=1, source_target_pairs={{0,4},{4,8},{8,12},{12,0},{1,5},{5,9},{9,13},{13,1},{2,6},{6,10},{... | collective-permute-start | bytes 1179656 | tf_op jit(solution)/shard_map/ppermute | solution.py:153
  62.3 3.4 %collective-permute-done.28.refs_2_ = bf16[384,256]{1,0:T(8,128)(2,1)S(1)} collective-permute-done((bf16[384,256]{1,0:T(8,128)(2,1)}, bf16[384,256]{1,0:T(8,128)(2,1)S(1)}, u32[]{:S(2)}, u32[]{:S(2)}) %collective-permute-start.28) | collective-permute-done | bytes 196640 | tf_op jit(solution)/shard_map/ppermute | solution.py:153
  65.9 8.3 %collective-permute-done.36.refs_0_ = bf16[384,256]{1,0:T(8,128)(2,1)S(1)} collective-permute-done((bf16[384,256]{1,0:T(8,128)(2,1)}, bf16[384,256]{1,0:T(8,128)(2,1)S(1)}, u32[]{:S(2)}, u32[]{:S(2)}) %collective-permute-start.36) | collective-permute-done | bytes 196640 | tf_op jit(solution)/shard_map/ppermute | solution.py:153
  77.7 2.8 %collective-permute-done.8.refs_6_ = bf16[32,2048]{1,0:T(8,128)(2,1)S(1)} collective-permute-done((bf16[32,2048]{1,0:T(8,128)(2,1)S(1)}, bf16[32,2048]{1,0:T(8,128)(2,1)S(1)}, u32[]{:S(2)}, u32[]{:S(2)}) %collective-permute-start.8) | collective-permute-done | bytes 131104 | tf_op jit(solution)/shard_map/ppermute | solution.py:157
  84.2 18.1 %collective-permute-done.14.refs_12_ = bf16[256,768]{1,0:T(8,128)(2,1)S(1)} collective-permute-done((bf16[256,768]{1,0:T(8,128)(2,1)S(1)}, bf16[256,768]{1,0:T(8,128)(2,1)S(1)}, u32[]{:S(2)}, u32[]{:S(2)}) %collective-permute-start.14) | collective-permute-done | bytes 393248 | tf_op jit(solution)/shard_map/ppermute | solution.py:153
  106.4 3.6 %collective-permute-done.30.refs_4_ = bf16[384,256]{1,0:T(8,128)(2,1)S(1)} collective-permute-done((bf16[384,256]{1,0:T(8,128)(2,1)S(1)}, bf16[384,256]{1,0:T(8,128)(2,1)S(1)}, u32[]{:S(2)}, u32[]{:S(2)}) %collective-permute-start.30) | collective-permute-done | bytes 196640 | tf_op jit(solution)/shard_map/ppermute | solution.py:157
  111.6 2.7 %collective-permute-done.38.refs_2_ = bf16[384,256]{1,0:T(8,128)(2,1)S(1)} collective-permute-done((bf16[384,256]{1,0:T(8,128)(2,1)S(1)}, bf16[384,256]{1,0:T(8,128)(2,1)S(1)}, u32[]{:S(2)}, u32[]{:S(2)}) %collective-permute-start.38) | collective-permute-done | bytes 196640 | tf_op jit(solution)/shard_map/ppermute | solution.py:157
  114.3 4.2 %collective-permute-done.42.refs_6_ = bf16[384,256]{1,0:T(8,128)(2,1)S(1)} collective-permute-done((bf16[384,256]{1,0:T(8,128)(2,1)S(1)}, bf16[384,256]{1,0:T(8,128)(2,1)S(1)}, u32[]{:S(2)}, u32[]{:S(2)}) %collective-permute-start.42) | collective-permute-done | bytes 196640 | tf_op jit(solution)/shard_map/ppermute | solution.py:157
  120.1 6.8 %collective-permute-done.11.refs_9_ = bf16[256,768]{1,0:T(8,128)(2,1)S(1)} collective-permute-done((bf16[256,768]{1,0:T(8,128)(2,1)S(1)}, bf16[256,768]{1,0:T(8,128)(2,1)S(1)}, u32[]{:S(2)}, u32[]{:S(2)}) %collective-permute-start.11) | collective-permute-done | bytes 393248 | tf_op jit(solution)/shard_map/ppermute | solution.py:157
  126.9 8.0 %collective-permute-done.15.refs_13_ = bf16[256,768]{1,0:T(8,128)(2,1)S(1)} collective-permute-done((bf16[256,768]{1,0:T(8,128)(2,1)S(1)}, bf16[256,768]{1,0:T(8,128)(2,1)S(1)}, u32[]{:S(2)}, u32[]{:S(2)}) %collective-permute-start.15) | collective-permute-done | bytes 393248 | tf_op jit(solution)/shard_map/ppermute | solution.py:157
  137.9 3.5 %shard_map.166 = (bf16[256,384]{1,0:T(8,128)(2,1)S(1)}, bf16[256,2048]{1,0:T(8,128)(2,1)S(1)}) custom-call(bf16[32,2048]{1,0:T(8,128)(2,1)S(1)} %get-tuple-element.39.refs_0_, bf16[32,2048]{1,0:T(8,128)(2,1)S(1)} %collective-permute-done.3.refs_1_, bf16[32,2048]{1,0:T(8,128)(2,1)S(1)} %collective-permute-done.4.refs_2_, ...), custom_call_target="tpu_custom_call" | custom-call | tf_op jit(solution)/shard_map/pallas_call | solution.py:468
  147.6 6.0 %collective-permute-done.32.b = bf16[128,1024]{1,0:T(8,128)(2,1)S(1)} collective-permute-done((bf16[128,1024]{1,0:T(8,128)(2,1)S(1)}, bf16[128,1024]{1,0:T(8,128)(2,1)S(1)}, u32[]{:S(2)}, u32[]{:S(2)}) %collective-permute-start.32) | collective-permute-done | bytes 262176 | tf_op jit(solution)/shard_map/ppermute | solution.py:157
  153.7 2.8 %collective-permute-start.34 = (bf16[32,1024]{1,0:T(8,128)(2,1)S(1)}, bf16[32,1024]{1,0:T(8,128)(2,1)S(1)}, u32[]{:S(2)}, u32[]{:S(2)}) collective-permute-start(bf16[32,1024]{1,0:T(8,128)(2,1)S(1)} %get-tuple-element.53), channel_id=1, source_target_pairs={{0,8},{4,12},{8,0},{12,4},{1,9},{5,13},{9,1},{13,5},{2,10},{6,14},... | collective-permute-start | bytes 196616 | tf_op jit(solution)/shard_map/ppermute | solution.py:153
  156.6 2.1 %collective-permute-done.44.b = bf16[128,1024]{1,0:T(8,128)(2,1)S(1)} collective-permute-done((bf16[128,1024]{1,0:T(8,128)(2,1)S(1)}, bf16[128,1024]{1,0:T(8,128)(2,1)S(1)}, u32[]{:S(2)}, u32[]{:S(2)}) %collective-permute-start.44) | collective-permute-done | bytes 262176 | tf_op jit(solution)/shard_map/ppermute | solution.py:157
  163.6 4.7 %collective-permute-done.46.refs_6_ = bf16[32,1024]{1,0:T(8,128)(2,1)S(1)} collective-permute-done((bf16[32,1024]{1,0:T(8,128)(2,1)S(1)}, bf16[32,1024]{1,0:T(8,128)(2,1)S(1)}, u32[]{:S(2)}, u32[]{:S(2)}) %collective-permute-start.46) | collective-permute-done | bytes 65568 | tf_op jit(solution)/shard_map/ppermute | solution.py:153
  (118 shorter events, 48.5 us)
Async XLA Ops:
  8.3 10.8 %collective-permute-start = (f32[2,1024]{1,0:T(2,128)S(1)}, f32[2,1024]{1,0:T(2,128)S(1)}, u32[]{:S(2)}, u32[]{:S(2)}) collective-permute-start(f32[2,1024]{1,0:T(2,128)S(1)} %get-tuple-element.37), channel_id=1, source_target_pairs={{0,4},{4,8},{8,12},{1,5},{5,9},{9,13},{2,6},{6,10},{10,14},{3,7},{... | collective-permute-start | bytes 24584 | tf_op jit(solution)/shard_map/ppermute | solution.py:336
  35.0 14.6 %collective-permute-start.4 = (bf16[32,2048]{1,0:T(8,128)(2,1)S(1)}, bf16[32,2048]{1,0:T(8,128)(2,1)S(1)}, u32[]{:S(2)}, u32[]{:S(2)}) collective-permute-start(bf16[32,2048]{1,0:T(8,128)(2,1)S(1)} %get-tuple-element.39.refs_0_), channel_id=1, source_target_pairs={{0,8},{4,12},{8,0},{12,4},{1,9},{5,13},{9,1},{13,5},{2,10},{6,14},... | collective-permute-start | bytes 393224 | tf_op jit(solution)/shard_map/ppermute | solution.py:153
  39.6 17.2 %collective-permute-start.5 = (bf16[32,2048]{1,0:T(8,128)(2,1)S(1)}, bf16[32,2048]{1,0:T(8,128)(2,1)S(1)}, u32[]{:S(2)}, u32[]{:S(2)}) collective-permute-start(bf16[32,2048]{1,0:T(8,128)(2,1)S(1)} %get-tuple-element.39.refs_0_), channel_id=1, source_target_pairs={{0,12},{4,0},{8,4},{12,8},{1,13},{5,1},{9,5},{13,9},{2,14},{6,2},{... | collective-permute-start | bytes 393224 | tf_op jit(solution)/shard_map/ppermute | solution.py:153
  39.8 20.4 %collective-permute-start.6 = (bf16[32,2048]{1,0:T(8,128)(2,1)S(1)}, bf16[32,2048]{1,0:T(8,128)(2,1)S(1)}, u32[]{:S(2)}, u32[]{:S(2)}) collective-permute-start(bf16[32,2048]{1,0:T(8,128)(2,1)S(1)} %get-tuple-element.39.refs_0_), channel_id=1, source_target_pairs={{0,2},{1,3},{2,0},{3,1},{4,6},{5,7},{6,4},{7,5},{8,10},{9,11},{10,... | collective-permute-start | bytes 393224 | tf_op jit(solution)/shard_map/ppermute | solution.py:157
  41.9 18.3 %collective-permute-start.12 = (bf16[256,384]{1,0:T(8,128)(2,1)}, bf16[256,384]{1,0:T(8,128)(2,1)S(1)}, u32[]{:S(2)}, u32[]{:S(2)}) collective-permute-start(bf16[256,384]{1,0:T(8,128)(2,1)} %get-tuple-element.41), channel_id=1, source_target_pairs={{0,12},{4,0},{8,4},{12,8},{1,13},{5,1},{9,5},{13,9},{2,14},{6,2},{... | collective-permute-start | bytes 589832 | tf_op jit(solution)/shard_map/ppermute | solution.py:153
  45.3 17.0 %collective-permute-start.16 = (bf16[256,384]{1,0:T(8,128)(2,1)}, bf16[256,384]{1,0:T(8,128)(2,1)S(1)}, u32[]{:S(2)}, u32[]{:S(2)}) collective-permute-start(bf16[256,384]{1,0:T(8,128)(2,1)} %get-tuple-element.43), channel_id=1, source_target_pairs={{0,12},{4,0},{8,4},{12,8},{1,13},{5,1},{9,5},{13,9},{2,14},{6,2},{... | collective-permute-start | bytes 589832 | tf_op jit(solution)/shard_map/ppermute | solution.py:153
  49.6 16.1 %collective-permute-start.28 = (bf16[384,256]{1,0:T(8,128)(2,1)}, bf16[384,256]{1,0:T(8,128)(2,1)S(1)}, u32[]{:S(2)}, u32[]{:S(2)}) collective-permute-start(bf16[384,256]{1,0:T(8,128)(2,1)} %get-tuple-element.48), channel_id=1, source_target_pairs={{0,4},{4,8},{8,12},{12,0},{1,5},{5,9},{9,13},{13,1},{2,6},{6,10},{... | collective-permute-start | bytes 589832 | tf_op jit(solution)/shard_map/ppermute | solution.py:153
  56.8 17.3 %collective-permute-start.36 = (bf16[384,256]{1,0:T(8,128)(2,1)}, bf16[384,256]{1,0:T(8,128)(2,1)S(1)}, u32[]{:S(2)}, u32[]{:S(2)}) collective-permute-start(bf16[384,256]{1,0:T(8,128)(2,1)} %get-tuple-element.55), channel_id=1, source_target_pairs={{0,8},{4,12},{8,0},{12,4},{1,9},{5,13},{9,1},{13,5},{2,10},{6,14},... | collective-permute-start | bytes 589832 | tf_op jit(solution)/shard_map/ppermute | solution.py:153
  60.2 14.1 %collective-permute-start.40 = (bf16[384,256]{1,0:T(8,128)(2,1)}, bf16[384,256]{1,0:T(8,128)(2,1)S(1)}, u32[]{:S(2)}, u32[]{:S(2)}) collective-permute-start(bf16[384,256]{1,0:T(8,128)(2,1)} %get-tuple-element.56), channel_id=1, source_target_pairs={{0,12},{4,0},{8,4},{12,8},{1,13},{5,1},{9,5},{13,9},{2,14},{6,2},{... | collective-permute-start | bytes 589832 | tf_op jit(solution)/shard_map/ppermute | solution.py:153
  60.2 23.4 %collective-permute-start.10 = (bf16[256,768]{1,0:T(8,128)(2,1)S(1)}, bf16[256,768]{1,0:T(8,128)(2,1)S(1)}, u32[]{:S(2)}, u32[]{:S(2)}) collective-permute-start(bf16[256,768]{1,0:T(8,128)(2,1)S(1)} %copy-done.15), channel_id=1, source_target_pairs={{0,4},{4,8},{8,12},{12,0},{1,5},{5,9},{9,13},{13,1},{2,6},{6,10},{... | collective-permute-start | bytes 1179656 | tf_op jit(solution)/shard_map/ppermute | solution.py:153
  62.3 40.0 %collective-permute-start.14 = (bf16[256,768]{1,0:T(8,128)(2,1)S(1)}, bf16[256,768]{1,0:T(8,128)(2,1)S(1)}, u32[]{:S(2)}, u32[]{:S(2)}) collective-permute-start(bf16[256,768]{1,0:T(8,128)(2,1)S(1)} %copy-done.14), channel_id=1, source_target_pairs={{0,8},{4,12},{8,0},{12,4},{1,9},{5,13},{9,1},{13,5},{2,10},{6,14},... | collective-permute-start | bytes 1179656 | tf_op jit(solution)/shard_map/ppermute | solution.py:153
  65.7 10.5 %collective-permute-start.7 = (bf16[32,2048]{1,0:T(8,128)(2,1)S(1)}, bf16[32,2048]{1,0:T(8,128)(2,1)S(1)}, u32[]{:S(2)}, u32[]{:S(2)}) collective-permute-start(bf16[32,2048]{1,0:T(8,128)(2,1)S(1)} %collective-permute-done.3.refs_1_), channel_id=1, source_target_pairs={{0,2},{1,3},{2,0},{3,1},{4,6},{5,7},{6,4},{7,5},{8,10},{9,11},{10,... | collective-permute-start | bytes 393224 | tf_op jit(solution)/shard_map/ppermute | solution.py:157
  80.5 25.4 %collective-permute-start.27 = (bf16[384,512]{1,0:T(8,128)(2,1)}, bf16[384,512]{1,0:T(8,128)(2,1)S(1)}, u32[]{:S(2)}, u32[]{:S(2)}) collective-permute-start(bf16[384,512]{1,0:T(8,128)(2,1)} %get-tuple-element.47.refs_0_), channel_id=1, source_target_pairs={{0,1},{1,0},{2,3},{3,2},{4,5},{5,4},{6,7},{7,6},{8,9},{9,8},{10,11... | collective-permute-start | bytes 1179656 | tf_op jit(solution)/shard_map/ppermute | solution.py:157
  82.1 20.2 %collective-permute-start.17 = (bf16[256,384]{1,0:T(8,128)(2,1)S(1)}, bf16[256,384]{1,0:T(8,128)(2,1)S(1)}, u32[]{:S(2)}, u32[]{:S(2)}) collective-permute-start(bf16[256,384]{1,0:T(8,128)(2,1)S(1)} %collective-permute-done.16.refs_14_), channel_id=1, source_target_pairs={{0,16},{16,0},{1,17},{17,1},{2,18},{18,2},{3,19},{19,3},{4,20},{20... | collective-permute-start | bytes 589832 | tf_op jit(solution)/shard_map/ppermute | solution.py:157
  83.6 20.2 %collective-permute-start.20 = (bf16[256,384]{1,0:T(8,128)(2,1)S(1)}, bf16[256,384]{1,0:T(8,128)(2,1)S(1)}, u32[]{:S(2)}, u32[]{:S(2)}) collective-permute-start(bf16[256,384]{1,0:T(8,128)(2,1)S(1)} %collective-permute-done.12.refs_10_), channel_id=1, source_target_pairs={{0,1},{1,0},{2,3},{3,2},{4,5},{5,4},{6,7},{7,6},{8,9},{9,8},{10,11... | collective-permute-start | bytes 589832 | tf_op jit(solution)/shard_map/ppermute | solution.py:157
  83.7 20.7 %collective-permute-start.24 = (bf16[256,384]{1,0:T(8,128)(2,1)S(1)}, bf16[256,384]{1,0:T(8,128)(2,1)S(1)}, u32[]{:S(2)}, u32[]{:S(2)}) collective-permute-start(bf16[256,384]{1,0:T(8,128)(2,1)S(1)} %collective-permute-done.16.refs_14_), channel_id=1, source_target_pairs={{0,1},{1,0},{2,3},{3,2},{4,5},{5,4},{6,7},{7,6},{8,9},{9,8},{10,11... | collective-permute-start | bytes 589832 | tf_op jit(solution)/shard_map/ppermute | solution.py:157
  103.8 10.5 %collective-permute-start.38 = (bf16[384,256]{1,0:T(8,128)(2,1)S(1)}, bf16[384,256]{1,0:T(8,128)(2,1)S(1)}, u32[]{:S(2)}, u32[]{:S(2)}) collective-permute-start(bf16[384,256]{1,0:T(8,128)(2,1)S(1)} %collective-permute-done.36.refs_0_), channel_id=1, source_target_pairs={{0,16},{16,0},{1,17},{17,1},{2,18},{18,2},{3,19},{19,3},{4,20},{20... | collective-permute-start | bytes 589832 | tf_op jit(solution)/shard_map/ppermute | solution.py:157
  104.3 14.2 %collective-permute-start.42 = (bf16[384,256]{1,0:T(8,128)(2,1)S(1)}, bf16[384,256]{1,0:T(8,128)(2,1)S(1)}, u32[]{:S(2)}, u32[]{:S(2)}) collective-permute-start(bf16[384,256]{1,0:T(8,128)(2,1)S(1)} %collective-permute-done.40.refs_4_), channel_id=1, source_target_pairs={{0,16},{16,0},{1,17},{17,1},{2,18},{18,2},{3,19},{19,3},{4,20},{20... | collective-permute-start | bytes 589832 | tf_op jit(solution)/shard_map/ppermute | solution.py:157
  105.9 29.6 %collective-permute-start.26 = (bf16[512,768]{1,0:T(8,128)(2,1)}, bf16[512,768]{1,0:T(8,128)(2,1)S(1)}, u32[]{:S(2)}, u32[]{:S(2)}) collective-permute-start(bf16[512,768]{1,0:T(8,128)(2,1)} %get-tuple-element.44.refs_16_), channel_id=1, source_target_pairs={{0,1},{1,0},{2,3},{3,2},{4,5},{5,4},{6,7},{7,6},{8,9},{9,8},{10,11... | collective-permute-start | bytes 2359304 | tf_op jit(solution)/shard_map/ppermute | solution.py:157
  105.9 21.1 %collective-permute-start.11 = (bf16[256,768]{1,0:T(8,128)(2,1)S(1)}, bf16[256,768]{1,0:T(8,128)(2,1)S(1)}, u32[]{:S(2)}, u32[]{:S(2)}) collective-permute-start(bf16[256,768]{1,0:T(8,128)(2,1)S(1)} %collective-permute-done.10.refs_8_), channel_id=1, source_target_pairs={{0,16},{16,0},{1,17},{17,1},{2,18},{18,2},{3,19},{19,3},{4,20},{20... | collective-permute-start | bytes 1179656 | tf_op jit(solution)/shard_map/ppermute | solution.py:157
  110.1 24.8 %collective-permute-start.15 = (bf16[256,768]{1,0:T(8,128)(2,1)S(1)}, bf16[256,768]{1,0:T(8,128)(2,1)S(1)}, u32[]{:S(2)}, u32[]{:S(2)}) collective-permute-start(bf16[256,768]{1,0:T(8,128)(2,1)S(1)} %collective-permute-done.14.refs_12_), channel_id=1, source_target_pairs={{0,16},{16,0},{1,17},{17,1},{2,18},{18,2},{3,19},{19,3},{4,20},{20... | collective-permute-start | bytes 1179656 | tf_op jit(solution)/shard_map/ppermute | solution.py:157
  118.5 16.4 %collective-permute-start.18 = (bf16[256,768]{1,0:T(8,128)(2,1)S(1)}, bf16[256,768]{1,0:T(8,128)(2,1)S(1)}, u32[]{:S(2)}, u32[]{:S(2)}) collective-permute-start(bf16[256,768]{1,0:T(8,128)(2,1)S(1)} %collective-permute-done.10.refs_8_), channel_id=1, source_target_pairs={{0,1},{1,0},{2,3},{3,2},{4,5},{5,4},{6,7},{7,6},{8,9},{9,8},{10,11... | collective-permute-start | bytes 1179656 | tf_op jit(solution)/shard_map/ppermute | solution.py:157
  119.9 15.5 %collective-permute-start.22 = (bf16[256,768]{1,0:T(8,128)(2,1)S(1)}, bf16[256,768]{1,0:T(8,128)(2,1)S(1)}, u32[]{:S(2)}, u32[]{:S(2)}) collective-permute-start(bf16[256,768]{1,0:T(8,128)(2,1)S(1)} %collective-permute-done.14.refs_12_), channel_id=1, source_target_pairs={{0,1},{1,0},{2,3},{3,2},{4,5},{5,4},{6,7},{7,6},{8,9},{9,8},{10,11... | collective-permute-start | bytes 1179656 | tf_op jit(solution)/shard_map/ppermute | solution.py:157
  145.7 13.0 %collective-permute-start.44 = (bf16[128,1024]{1,0:T(8,128)(2,1)S(1)}, bf16[128,1024]{1,0:T(8,128)(2,1)S(1)}, u32[]{:S(2)}, u32[]{:S(2)}) collective-permute-start(bf16[128,1024]{1,0:T(8,128)(2,1)S(1)} %get-tuple-element.58), channel_id=1, source_target_pairs={{0,2},{1,3},{2,0},{3,1},{4,6},{5,7},{6,4},{7,5},{8,10},{9,11},{10,... | collective-permute-start | bytes 786440 | tf_op jit(solution)/shard_map/ppermute | solution.py:157
  (40 other events, 252.8 us)
